TPU v7x, 32 devices: a whole 2x2x4 slice. The times are simulated.
32 devices in a mesh: grp: 2 (over y), sp: 4 (over z), tp: 4 (over x, core).
Axes of the slice: x: 2, y: 2, z: 4, core: 2. Of those that a mesh axis runs over, the one named last changes fastest.
Arguments:
- window_query: bfloat16 [2560, 2048], P(('grp', 'sp'), 'tp'), parts along dimension 0, may hold values from -24 to 24
- window_key: bfloat16 [2560, 1024], P(('grp', 'sp'), 'tp'), parts along dimension 0, may hold values from -24 to 24
- window_value: bfloat16 [2560, 1024], P(('grp', 'sp'), 'tp'), parts along dimension 0, may hold values from -6 to 6
- grid_query: bfloat16 [2560, 2048], P(('grp', 'sp'), 'tp'), parts along dimension 0, may hold values from -10 to 10
- grid_key: bfloat16 [2560, 1024], P(('grp', 'sp'), 'tp'), parts along dimension 0, may hold values from -10 to 10
- grid_value: bfloat16 [2560, 1024], P(('grp', 'sp'), 'tp'), parts along dimension 0, may hold values from -6 to 6
- sink_logit: float32 [16], P('tp'), may hold values from 1 to 6
- query_gain: float32 [128], replicated, may hold values from 0.8 to 6
- key_gain: float32 [128], replicated, may hold values from 0.8 to 6
- window_weights: bfloat16 [2048, 4096], P('tp'), may hold values from -0.59765625 to 0.59765625
- grid_weights: bfloat16 [2048, 4096], P('tp'), may hold values from -0.59765625 to 0.59765625
Outputs:
- merged: bfloat16 [2560, 4096], P(('grp', 'sp', 'tp')), parts along dimension 0
There are 2 independent parts, one for each index of `grp`. A program takes and returns all parts, laid end to end along the dimension named above; an argument that names none is the same for every part. Nothing has to cross between parts.
All inputs are finite; a program needn't handle non-finite values.
Results may differ from a plain program's by a relative error of at most 0.014.
The roundings to bfloat16 on the way count: a program that leaves them out, or rounds other values in their place, can miss the bound.
Values may be sent and summed in bfloat16 or wider, within the bound.
A program may use at most 64 MiB of HBM per device.

v0:
```python
import jax
import jax.numpy as jnp
from jax import lax
from jax.sharding import PartitionSpec as P

HEAD = 128
QH_A = 16
WINDOW = 128
GRID_W = 64


THETA = 10000.0
NEGATIVE = -1e30
EPSILON = 1e-06


def extended(cells, sides, width):
    for axis, dim in sides:
        count = lax.axis_size(axis)
        ends = count - 1
        head = lax.slice_in_dim(cells, 0, width, axis=dim)
        tail = lax.slice_in_dim(cells, cells.shape[dim] - width, cells.shape[dim], axis=dim)
        cells = jnp.concatenate(
            [
                lax.ppermute(tail, axis, [(i, (i + 1) % count) for i in range(ends)]),
                cells,
                lax.ppermute(head, axis, [((i + 1) % count, i) for i in range(ends)]),
            ],
            axis=dim,
        )
    return cells


def turn_section(values, places):
    width = values.shape[-1]
    half_width = width // 2
    frequency = THETA ** (-jnp.arange(0, width, 2, dtype=jnp.float32) / width)
    angles = places[:, None] * frequency[None, :]
    cosine = jnp.cos(angles)[:, None, :]
    sine_part = jnp.sin(angles)[:, None, :]
    first_half = values[..., :half_width]
    second_half = values[..., half_width:]
    return jnp.concatenate(
        [
            first_half * cosine - second_half * sine_part,
            second_half * cosine + first_half * sine_part,
        ],
        axis=-1,
    )


def normed_turn(values, gain, places):
    count_rows = values.shape[0]
    shaped = values.astype(jnp.float32).reshape(count_rows, -1, HEAD)
    scaled = shaped * lax.rsqrt(jnp.mean(shaped * shaped, axis=-1, keepdims=True) + EPSILON)
    scaled = scaled * gain
    grid_row = (places // GRID_W).astype(jnp.float32)
    grid_col = (places % GRID_W).astype(jnp.float32)
    section = HEAD // 2
    turned = jnp.concatenate(
        [
            turn_section(scaled[..., :section], grid_row),
            turn_section(scaled[..., section:], grid_col),
        ],
        axis=-1,
    )
    return turned.astype(jnp.bfloat16)


def window_attend(queries, keys_pad, values_pad, slopes, sink_logits, offset, total_rows):
    query_rows = queries.shape[0]
    block_span = WINDOW // 2
    blocks = query_rows // block_span
    key_heads = keys_pad.shape[1] // HEAD
    group_size = queries.shape[1] // keys_pad.shape[1]
    query_blocks = queries.reshape(blocks, block_span, key_heads, group_size, HEAD)
    key_blocks = keys_pad.reshape(blocks + 4, block_span, key_heads, HEAD)
    value_blocks = values_pad.reshape(blocks + 4, block_span, key_heads, HEAD)
    key_window = jnp.concatenate(
        [key_blocks[block_shift : block_shift + blocks] for block_shift in range(5)], axis=1
    )
    value_window = jnp.concatenate(
        [value_blocks[block_shift : block_shift + blocks] for block_shift in range(5)], axis=1
    )
    scores = jnp.einsum(
        "nqkgd,nskd->kgnqs", query_blocks, key_window, preferred_element_type=jnp.float32
    ) * HEAD ** (-0.5)
    query_place = offset + jnp.arange(query_rows, dtype=jnp.int32).reshape(blocks, block_span, 1)
    key_place = (
        offset
        - WINDOW
        + block_span * jnp.arange(blocks, dtype=jnp.int32)[:, None, None]
        + jnp.arange(5 * block_span, dtype=jnp.int32)[None, None, :]
    )
    distance = jnp.abs(key_place - query_place)
    inside = (distance <= WINDOW) & (key_place >= 0) & (key_place < total_rows)
    slope_grid = slopes.reshape(key_heads, group_size, 1, 1, 1)
    sink_grid = sink_logits.reshape(key_heads, group_size, 1, 1)
    scores = jnp.where(inside, scores - slope_grid * distance.astype(jnp.float32), NEGATIVE)
    highest = jnp.maximum(jnp.max(scores, axis=-1), sink_grid)
    raised = jnp.exp(scores - highest[..., None])
    denominator = jnp.sum(raised, axis=-1) + jnp.exp(sink_grid - highest)
    weights = (raised / denominator[..., None]).astype(jnp.bfloat16)
    attended = jnp.einsum(
        "kgnqs,nskd->nqkgd", weights, value_window, preferred_element_type=jnp.float32
    )
    return attended.astype(jnp.bfloat16).reshape(query_rows, -1)


def absorb_keys(carry, queries, key_block, value_block):
    highest, summed, gathered = carry
    scores = jnp.einsum(
        "tkgd,skd->kgts", queries, key_block, preferred_element_type=jnp.float32
    ) * HEAD ** (-0.5)
    raised_top = jnp.maximum(highest, jnp.max(scores, axis=-1))
    fading = jnp.exp(highest - raised_top)
    raised = jnp.exp(scores - raised_top[..., None])
    summed = summed * fading + jnp.sum(raised, axis=-1)
    gathered = gathered * fading[..., None] + jnp.einsum(
        "kgts,skd->kgtd",
        raised.astype(jnp.bfloat16),
        value_block,
        preferred_element_type=jnp.float32,
    )
    return (raised_top, summed, gathered)


def sweep_keys(carry, queries, key_rows, value_rows):
    count_rows = key_rows.shape[0]
    block_rows = count_rows
    while block_rows > 1024 and block_rows % 2 == 0:
        block_rows = block_rows // 2
    key_heads = queries.shape[1]
    key_blocks = key_rows.reshape(count_rows // block_rows, block_rows, key_heads, HEAD)
    value_blocks = value_rows.reshape(count_rows // block_rows, block_rows, key_heads, HEAD)

    def scan_step(inner, block_pair):
        return (absorb_keys(inner, queries, block_pair[0], block_pair[1]), None)

    result, _ = lax.scan(scan_step, carry, (key_blocks, value_blocks))
    return result


def per_device(
    window_query,
    window_key,
    window_value,
    grid_query,
    grid_key,
    grid_value,
    sink_logit,
    query_gain,
    key_gain,
    window_weights,
    grid_weights,
):
    local_rows = window_query.shape[0]
    offset = lax.axis_index("sp") * local_rows
    total_rows = local_rows * lax.axis_size("sp")
    local_heads = sink_logit.shape[0]
    head_number = lax.axis_index("tp") * local_heads + 1 + jnp.arange(local_heads, dtype=jnp.int32)
    slopes = 2.0 ** (-8.0 * head_number.astype(jnp.float32) / QH_A)
    stacked = jnp.stack([window_key, window_value])
    padded = extended(stacked, (("sp", 1),), WINDOW)
    window_out = window_attend(
        window_query, padded[0], padded[1], slopes, sink_logit, offset, total_rows
    )
    places = offset + jnp.arange(local_rows, dtype=jnp.int32)
    key_heads = grid_key.shape[1] // HEAD
    group_size = grid_query.shape[1] // grid_key.shape[1]
    turned_q = normed_turn(grid_query, query_gain, places).reshape(
        local_rows, key_heads, group_size, HEAD
    )
    turned_k = normed_turn(grid_key, key_gain, places).reshape(local_rows, key_heads * HEAD)
    start_carry = (
        jnp.full((key_heads, group_size, local_rows), NEGATIVE, jnp.float32),
        jnp.zeros((key_heads, group_size, local_rows), jnp.float32),
        jnp.zeros((key_heads, group_size, local_rows, HEAD), jnp.float32),
    )
    final_carry = sweep_keys(
        start_carry,
        turned_q,
        lax.all_gather(turned_k, "sp", axis=0, tiled=True),
        lax.all_gather(grid_value, "sp", axis=0, tiled=True),
    )
    grid_out = (final_carry[2] / final_carry[1][..., None]).astype(jnp.bfloat16)
    shaped_b = grid_weights.reshape(key_heads, group_size, HEAD, grid_weights.shape[1])
    projected = jnp.dot(window_out, window_weights, preferred_element_type=jnp.float32)
    return lax.psum_scatter(
        (
            projected
            + jnp.einsum("kgtd,kgdo->to", grid_out, shaped_b, preferred_element_type=jnp.float32)
        ).astype(jnp.bfloat16),
        "tp",
        scatter_dimension=0,
        tiled=True,
    )


def solution(mesh):
    return jax.shard_map(
        per_device,
        mesh=mesh,
        in_specs=(
            P(("grp", "sp"), "tp"),
            P(("grp", "sp"), "tp"),
            P(("grp", "sp"), "tp"),
            P(("grp", "sp"), "tp"),
            P(("grp", "sp"), "tp"),
            P(("grp", "sp"), "tp"),
            P("tp"),
            P(),
            P(),
            P("tp", None),
            P("tp", None),
        ),
        out_specs=P(("grp", "sp", "tp"), None),
        check_vma=False,
    )
```

profile of v0, /device:TPU:0, one launch (start us, length us, event | category | flops | bytes accessed | tf_op | source)
XLA Modules:
  0.0 126.3 jit_solution(11127519755207074489)
XLA Ops:
  6.5 1.7 %pad_maximum_fusion.3 = (bf16[2,128,256]{2,1,0:T(8,128)(2,1)}, bf16[2,128,256]{2,1,0:T(8,128)(2,1)}) fusion(bf16[1,320,256]{2,1,0:T(8,128)(2,1)} %bitcast.74, bf16[1,320,256]{2,1,0:T(8,128)(2,1)} %bitcast.76), kind=kLoop, calls=%fused_computation.76 | loop fusion | flops 524288 | bytes 589824 | tf_op jit(solution)/shard_map/stack | solution.py:163
  8.2 1.3 %collective-permute-start.1 = (bf16[2,128,256]{2,1,0:T(8,128)(2,1)}, bf16[2,128,256]{2,1,0:T(8,128)(2,1)S(1)}, u32[]{:S(2)}, u32[]{:S(2)}) collective-permute-start(bf16[2,128,256]{2,1,0:T(8,128)(2,1)} %get-tuple-element.137), channel_id=1, source_target_pairs={{4,0},{8,4},{12,8},{5,1},{9,5},{13,9},{6,2},{10,6},{14,10},{7,3},{... | collective-permute-start | bytes 393224 | tf_op jit(solution)/shard_map/ppermute | solution.py:27
  9.5 5.6 %collective-permute-start = (bf16[2,128,256]{2,1,0:T(8,128)(2,1)}, bf16[2,128,256]{2,1,0:T(8,128)(2,1)S(1)}, u32[]{:S(2)}, u32[]{:S(2)}) collective-permute-start(bf16[2,128,256]{2,1,0:T(8,128)(2,1)} %get-tuple-element.138), channel_id=1, source_target_pairs={{0,4},{4,8},{8,12},{1,5},{5,9},{9,13},{2,6},{6,10},{10,14},{3,7},{... | collective-permute-start | bytes 393224 | tf_op jit(solution)/shard_map/ppermute | solution.py:25
  15.1 0.6 add_add_fusion
  15.8 0.7 fusion.29
  16.4 0.7 iota_add_fusion
  17.1 1.1 reshape.331
  18.6 1.1 multiply_multiply_fusion.1
  19.7 1.2 multiply_cosine_fusion.1
  20.9 1.1 subtract_convert_fusion.3
  22.1 1.0 pad_maximum_fusion.2
  23.1 17.3 %all_gather.6 = bf16[1280,256]{1,0:T(8,128)(2,1)S(1)} all-gather(bf16[320,256]{1,0:T(8,128)(2,1)S(1)} %bitcast.83), channel_id=1, replica_groups=mesh['grp'=2,'sp'=4,'tp'=4] {'sp'}, dimensions={0}, use_global_device_ids=true | all-gather | bytes 819200 | tf_op jit(solution)/shard_map/all_gather | solution.py:183
  41.6 1.1 subtract_convert_fusion.1
  42.8 0.8 copy.100
  43.6 0.8 copy.99
  44.4 16.7 %all_gather.7 = bf16[1280,256]{1,0:T(8,128)(2,1)S(1)} all-gather(bf16[320,256]{1,0:T(8,128)(2,1)S(1)} %copy-done.4), channel_id=1, replica_groups=mesh['grp'=2,'sp'=4,'tp'=4] {'sp'}, dimensions={0}, use_global_device_ids=true | all-gather | bytes 819200 | tf_op jit(solution)/shard_map/all_gather | solution.py:184
  61.3 1.5 %pad_maximum_fusion.1 = bf16[320,2,2,128]{3,0,2,1:T(8,128)(2,1)S(1)} fusion(bf16[320,2,2,32]{3,0,2,1:T(8,128)(2,1)} %bitcast.80, bf16[320,2,2,32]{3,0,2,1:T(8,128)(2,1)} %bitcast.81, bf16[320,2,2,32]{3,0,2,1:T(8,128)(2,1)S(1)} %bitcast.79, bf16[320,2,2,32]{3,0,2,1:T(8,128)(2,1)S(1)} %bitcast.78), kind=kLoop, calls=%fused_computation.49 | loop fusion | flops 1310720 | bytes 655360 | tf_op jit(solution)/shard_map/concatenate | solution.py:60
  62.8 6.5 %while.15 = (s32[]{:T(128)}, f32[2,2,320]{2,1,0:T(2,128)S(1)}, f32[2,2,320]{2,1,0:T(2,128)S(1)}, f32[2,2,320,128]{3,2,1,0:T(8,128)S(1)}, bf16[2,640,2,128]{3,2,1...) while((s32[]{:T(128)}, f32[2,2,320]{2,1,0:T(2,128)S(1)}, ...), condition=%wide.region_7.8_spmd.clone, body=%wide.region_4.7_spmd.clone.sunk | while | flops 426481920 | bytes 13516917 | solution.py:140
  62.8 0.5 constant_dynamic-slice_fusion.3
  63.3 0.7 bitcast_reduce_fusion.2
  64.0 1.0 fusion.50
  65.0 1.0 fusion.52
  66.1 0.5 constant_dynamic-slice_fusion.3
  66.5 0.7 bitcast_reduce_fusion.2
  67.3 1.0 fusion.50
  68.3 1.0 fusion.52
  69.6 5.7 %convolution_bitcast_fusion = f32[320,4096]{1,0:T(8,128)} fusion(bf16[2,2,128,4096]{3,2,1,0:T(8,128)(2,1)} %bitcast.84, f32[2,2,320,128]{3,2,1,0:T(8,128)S(1)} %get-tuple-element.43, f32[2,2,320]{2,1,0:T(2,128)S(1)} %get-tuple-element.44), kind=kOutput, calls=%fused_computation.21 | convolution fusion | flops 1342504960 | bytes 10097664 | tf_op jit(solution)/shard_map/kgtd,kgdo->to/dot_general | solution.py:192
  76.7 0.8 fusion.37
  77.5 0.7 fusion.17
  78.5 0.6 fusion.18
  79.6 6.8 %fusion.14 = bf16[320,4096]{1,0:T(8,128)(2,1)} fusion(f32[320,4096]{1,0:T(8,128)} %convolution_bitcast_fusion, bf16[320,512]{1,0:T(8,128)(2,1)S(1)} %reshape.322, bf16[512,4096]{1,0:T(8,128)(2,1)} %param.22), kind=kOutput, calls=%fused_computation.23 | convolution fusion | flops 1344798720 | bytes 12386304 | tf_op jit(solution)/shard_map/dot_general | solution.py:188
  86.4 33.1 %reduce-scatter.2.cloned.1.call-done = bf16[80,4096]{1,0:T(8,128)(2,1)} async-done(((bf16[320,4096]{1,0:T(8,128)(2,1)}), bf16[80,4096]{1,0:T(8,128)(2,1)}) %reduce-scatter.2.cloned.1.call-update) | async-done | bytes 655376 | tf_op jit(solution)/shard_map/reduce_scatter | solution.py:189
  (80 shorter events, 4.3 us)
Async XLA Ops:
  6.5 112.9 %reduce-scatter.2.cloned.1.call-start = ((), (), s32[]{:S(2)}) async-start(), calls=%async_computation.1 | async-start | bytes 3276800 | tf_op jit(solution)/shard_map/reduce_scatter | solution.py:189
  8.2 67.6 %collective-permute-start.1 = (bf16[2,128,256]{2,1,0:T(8,128)(2,1)}, bf16[2,128,256]{2,1,0:T(8,128)(2,1)S(1)}, u32[]{:S(2)}, u32[]{:S(2)}) collective-permute-start(bf16[2,128,256]{2,1,0:T(8,128)(2,1)} %get-tuple-element.137), channel_id=1, source_target_pairs={{4,0},{8,4},{12,8},{5,1},{9,5},{13,9},{6,2},{10,6},{14,10},{7,3},{... | collective-permute-start | bytes 393224 | tf_op jit(solution)/shard_map/ppermute | solution.py:27
  9.5 66.3 %collective-permute-start = (bf16[2,128,256]{2,1,0:T(8,128)(2,1)}, bf16[2,128,256]{2,1,0:T(8,128)(2,1)S(1)}, u32[]{:S(2)}, u32[]{:S(2)}) collective-permute-start(bf16[2,128,256]{2,1,0:T(8,128)(2,1)} %get-tuple-element.138), channel_id=1, source_target_pairs={{0,4},{4,8},{8,12},{1,5},{5,9},{9,13},{2,6},{6,10},{10,14},{3,7},{... | collective-permute-start | bytes 393224 | tf_op jit(solution)/shard_map/ppermute | solution.py:25
  19.7 20.8 %copy-start.3 = (bf16[320,512]{1,0:T(8,128)(2,1)S(1)}, bf16[320,512]{1,0:T(8,128)(2,1)}, u32[]{:S(2)}) copy-start(bf16[320,512]{1,0:T(8,128)(2,1)} %param.16) | copy-start | bytes 983044
  22.0 19.1 %copy-start.9 = (f32[128]{0:T(128)S(1)}, f32[128]{0:T(128)}, u32[]{:S(2)}) copy-start(f32[128]{0:T(128)} %param.20) | copy-start | bytes 1540
  41.6 2.8 %copy-start.4 = (bf16[320,256]{1,0:T(8,128)(2,1)S(1)}, bf16[320,256]{1,0:T(8,128)(2,1)}, u32[]{:S(2)}) copy-start(bf16[320,256]{1,0:T(8,128)(2,1)} %param.18) | copy-start | bytes 491524
  62.8 6.6 %copy-start.5 = (s32[5,320]{1,0:T(8,128)S(1)}, s32[5,320]{1,0:T(8,128)}, u32[]{:S(2)}) copy-start(s32[5,320]{1,0:T(8,128)} %iota_add_fusion) | copy-start | bytes 19204
  62.8 6.6 %copy-start.6 = (s32[5,64]{1,0:T(8,128)S(1)}, s32[5,64]{1,0:T(8,128)}, u32[]{:S(2)}) copy-start(s32[5,64]{1,0:T(8,128)} %add_add_fusion) | copy-start | bytes 3844
  69.5 5.8 %copy-start.7 = (pred[5,320]{1,0:T(8,128)(4,1)S(1)}, pred[5,320]{1,0:T(8,128)(4,1)}, u32[]{:S(2)}) copy-start(pred[5,320]{1,0:T(8,128)(4,1)} %get-tuple-element.145) | copy-start | bytes 4804
  69.5 5.8 %copy-start.8 = (pred[5,320]{1,0:T(8,128)(4,1)S(1)}, pred[5,320]{1,0:T(8,128)(4,1)}, u32[]{:S(2)}) copy-start(pred[5,320]{1,0:T(8,128)(4,1)} %get-tuple-element.146) | copy-start | bytes 4804
  69.5 6.0 %copy-start.1 = (bf16[320,256]{1,0:T(8,128)(2,1)S(1)}, bf16[320,256]{1,0:T(8,128)(2,1)}, u32[]{:S(2)}) copy-start(bf16[320,256]{1,0:T(8,128)(2,1)} %param.14) | copy-start | bytes 491524
  69.5 6.0 %copy-start = (bf16[320,256]{1,0:T(8,128)(2,1)S(1)}, bf16[320,256]{1,0:T(8,128)(2,1)}, u32[]{:S(2)}) copy-start(bf16[320,256]{1,0:T(8,128)(2,1)} %param.15) | copy-start | bytes 491524
  69.6 6.1 %copy-start.10 = (f32[4]{0:T(128)S(1)}, f32[4]{0:T(128)}, u32[]{:S(2)}) copy-start(f32[4]{0:T(128)} %param.19) | copy-start | bytes 52
  69.6 6.2 %copy-start.2 = (bf16[320,512]{1,0:T(8,128)(2,1)S(1)}, bf16[320,512]{1,0:T(8,128)(2,1)}, u32[]{:S(2)}) copy-start(bf16[320,512]{1,0:T(8,128)(2,1)} %param.13) | copy-start | bytes 983044
Sparse Core Ops, SparseCore 0:
  86.5 32.8 reduce-scatter.1
where the time goes:
time: 127 us; the launch traced here: 126 us
  blocking collectives  34 us (27%)
  waiting for transfers between devices  33.1 us (26%)
  matrix products  17.3 us (14%)
  other arithmetic  15.2 us (12%)
  between operations  13.9 us (11%)
  starting transfers between devices  6.87 us (5%)
  local copies, waits for them, and re-layouts  5.81 us (5%)
    reduce_scatter x1, waiting for transfers between devices, per_device(): lax.psum_scatter((projected + jnp.einsum('kgtd,kgdo->to', grid_out, shape...  33.1 us
    all_gather x1, blocking collectives, per_device(): lax.all_gather(turned_k, 'sp', axis=0, tiled=True)  17.3 us
    all_gather x1, blocking collectives, per_device(): lax.all_gather(grid_value, 'sp', axis=0, tiled=True)  16.7 us
    dot_general x1, matrix products, per_device(): jnp.dot(window_out, window_weights, preferred_element_type=jnp.float32)  6.78 us
    dot_general x1, matrix products, per_device(): jnp.einsum('kgtd,kgdo->to', grid_out, shaped_b, preferred_element_type=jn...  5.7 us
    ppermute x1, starting transfers between devices, extended(): lax.ppermute(tail, axis, [(i, (i + 1) % count) for i in range(ends)])  5.59 us
  transfers between devices with their start and end apart: 3, of which 1 were waited for; matrix products, arithmetic and copies ran while one was open for 21% of the time, Pallas kernels for 0%

commit v1 on v0

v1 whole, which is shorter than its diff:
```python
import functools
import math

import jax
import jax.numpy as jnp
from jax import lax
from jax.experimental import pallas as pl
from jax.experimental.pallas import tpu as pltpu
from jax.sharding import PartitionSpec as P

HEAD = 128
QH_A = 16
WINDOW = 128
GRID_W = 64
THETA = 10000.0
NEGATIVE = -1e30
EPSILON = 1e-06
MESH = pl.DeviceIdType.MESH
F32 = jnp.float32
BF16 = jnp.bfloat16


def dot_nt(a, b):
    return lax.dot_general(a, b, (((1,), (1,)), ((), ())), preferred_element_type=F32)


def dot_tn(a, b):
    return lax.dot_general(a, b, (((0,), (0,)), ((), ())), preferred_element_type=F32)


def kernel(
    n, n_tp, rows, kvh, group, chunks,
    wq_hbm, wk_hbm, wv_hbm, gq_hbm, gk_hbm, gv_hbm, sink_ref, qgain_ref, kgain_ref, ww_hbm, gw_hbm,
    out_ref,
    qw, wkv, qraw, kraw, qg, kvbuf, ww, gw, cosine, sine, top, total, acc, attn, proj, pbuf, dbuf, sbuf, rbuf, own,
    lsem, gsend, grecv, hsend, hrecv, dsend, drecv, xsend, xrecv,
):
    me = lax.axis_index("sp")
    t = lax.axis_index("tp")
    core = lax.rem(t, 2)
    x = t // 2
    n_x = n_tp // 2
    partner = x * 2 + 1 - core
    out_rows = rows // n_tp
    width = ww.shape[1] // chunks
    span = group * rows
    has_left = me > 0
    has_right = me < n - 1

    loads = []

    def load(src, dst):
        copy = pltpu.make_async_copy(src, dst, lsem.at[len(loads)])
        copy.start()
        loads.append(copy)
        return copy

    def head_cols(h):
        return slice(h * HEAD, (h + 1) * HEAD)

    k_loads = [load(gk_hbm.at[:, head_cols(g)], kraw.at[g]) for g in range(kvh)]
    v_loads = [load(gv_hbm.at[:, head_cols(g)], kvbuf.at[me, g, 1]) for g in range(kvh)]
    w_loads = []
    for g in range(kvh):
        w_loads.append(load(wk_hbm.at[:, head_cols(g)], wkv.at[g, 0, WINDOW : WINDOW + rows]))
        w_loads.append(load(wv_hbm.at[:, head_cols(g)], wkv.at[g, 1, WINDOW : WINDOW + rows]))
    q_loads = []
    for g in range(kvh):
        for u in range(group):
            q_loads.append(load(gq_hbm.at[:, head_cols(g * group + u)], qraw.at[g, u * rows : (u + 1) * rows]))
    wq_loads = []
    for g in range(kvh):
        for u in range(group):
            wq_loads.append(load(wq_hbm.at[:, head_cols(g * group + u)], qw.at[g, u * rows : (u + 1) * rows]))
    ww_load = load(ww_hbm, ww)
    gw_load = load(gw_hbm, gw)

    barrier = pltpu.get_barrier_semaphore()

    def greet(device):
        pl.semaphore_signal(barrier, inc=1, device_id=device, device_id_type=MESH)

    @pl.when(has_left)
    def _():
        greet({"sp": me - 1})

    @pl.when(has_right)
    def _():
        greet({"sp": me + 1})

    greet({"tp": partner})
    for dx in range(1, n_x):
        greet({"tp": lax.rem(x + dx, n_x) * 2 + core})

    place = me * rows + lax.broadcasted_iota(jnp.int32, (rows, HEAD), 0)
    lane = lax.broadcasted_iota(jnp.int32, (rows, HEAD), 1)
    section = HEAD // 2
    half = section // 2
    frequency = jnp.exp(jnp.bitwise_and(lane, half - 1).astype(F32) * (-2.0 * math.log(THETA) / section))
    position = jnp.where(lane < section, place // GRID_W, lax.rem(place, GRID_W)).astype(F32)
    angle = position * frequency
    low = jnp.bitwise_and(lane, section - 1) < half
    cosine[...] = jnp.cos(angle)
    sine[...] = jnp.where(low, -jnp.sin(angle), jnp.sin(angle))

    def turn(values, gain):
        v = values.astype(F32)
        v = v * lax.rsqrt(jnp.mean(v * v, axis=1, keepdims=True) + EPSILON) * gain
        first = lax.broadcasted_iota(jnp.int32, v.shape, 1)
        other = jnp.where(
            jnp.bitwise_and(first, section - 1) < half,
            pltpu.roll(v, HEAD - half, 1),
            pltpu.roll(v, half, 1),
        )
        return (v * cosine[...] + other * sine[...]).astype(BF16)

    for g in range(kvh):
        k_loads[g].wait()
        kvbuf[me, g, 0] = turn(kraw[g], kgain_ref[...])
    for copy in v_loads:
        copy.wait()

    pl.semaphore_wait(barrier, has_left.astype(jnp.int32) + has_right.astype(jnp.int32) + n_x)

    def block_copy(source, g, direction):
        return pltpu.make_async_remote_copy(
            src_ref=kvbuf.at[source, g],
            dst_ref=kvbuf.at[source, g],
            send_sem=gsend.at[direction, source, g],
            recv_sem=grecv.at[source, g],
            device_id={"sp": me + 1 if direction == 0 else me - 1},
            device_id_type=MESH,
        )

    def halo_copy(direction):
        source = rows if direction == 0 else WINDOW
        target = 0 if direction == 0 else WINDOW + rows
        return pltpu.make_async_remote_copy(
            src_ref=wkv.at[:, :, source : source + WINDOW],
            dst_ref=wkv.at[:, :, target : target + WINDOW],
            send_sem=hsend.at[direction],
            recv_sem=hrecv.at[direction],
            device_id={"sp": me + 1 if direction == 0 else me - 1},
            device_id_type=MESH,
        )

    for g in range(kvh):
        @pl.when(has_right)
        def _():
            block_copy(me, g, 0).start()

        @pl.when(has_left)
        def _():
            block_copy(me, g, 1).start()

    for copy in w_loads:
        copy.wait()

    @pl.when(has_right)
    def _():
        halo_copy(0).start()

    @pl.when(has_left)
    def _():
        halo_copy(1).start()

    @pl.when(jnp.logical_not(has_left))
    def _():
        wkv[:, :, 0:WINDOW] = jnp.zeros((kvh, 2, WINDOW, HEAD), BF16)

    @pl.when(jnp.logical_not(has_right))
    def _():
        wkv[:, :, WINDOW + rows :] = jnp.zeros((kvh, 2, WINDOW, HEAD), BF16)

    for copy in q_loads:
        copy.wait()
    for g in range(kvh):
        for u in range(group):
            part = slice(u * rows, (u + 1) * rows)
            qg[g, part] = turn(qraw[g, part], qgain_ref[...])

    scale = HEAD ** (-0.5)

    def absorb(source, g, first=False):
        scores = dot_nt(kvbuf[source, g, 0], qg[g]) * scale
        block_top = jnp.max(scores, axis=0, keepdims=True)
        if first:
            raised = jnp.exp(scores - block_top)
            top[g] = block_top
            total[g] = jnp.sum(raised, axis=0, keepdims=True)
            acc[g] = dot_tn(kvbuf[source, g, 1], raised.astype(BF16))
        else:
            before = top[g]
            new_top = jnp.maximum(before, block_top)
            fading = jnp.exp(before - new_top)
            raised = jnp.exp(scores - new_top)
            top[g] = new_top
            total[g] = total[g] * fading + jnp.sum(raised, axis=0, keepdims=True)
            acc[g] = acc[g] * fading + dot_tn(kvbuf[source, g, 1], raised.astype(BF16))

    for g in range(kvh):
        absorb(me, g, True)

    def relay(d):
        for g in range(kvh):
            @pl.when(me - d >= 0)
            def _():
                block_copy(me - d, g, 0).wait_recv()

                @pl.when(has_right)
                def _():
                    block_copy(me - d, g, 0).start()

            @pl.when(me + d < n)
            def _():
                block_copy(me + d, g, 1).wait_recv()

                @pl.when(has_left)
                def _():
                    block_copy(me + d, g, 1).start()

            @pl.when(me - d >= 0)
            def _():
                absorb(me - d, g)

            @pl.when(me + d < n)
            def _():
                absorb(me + d, g)

    def put_heads(base, g, value):
        turned = jnp.transpose(value).astype(BF16)
        for u in range(group):
            attn[:, base + (g * group + u) * HEAD : base + (g * group + u + 1) * HEAD] = turned[u * rows : (u + 1) * rows]

    heads_width = kvh * group * HEAD

    def windowed():
        for copy in wq_loads:
            copy.wait()

        @pl.when(has_left)
        def _():
            halo_copy(0).wait_recv()

        @pl.when(has_right)
        def _():
            halo_copy(1).wait_recv()

        padded = rows + 2 * WINDOW
        key_at = lax.broadcasted_iota(jnp.int32, (padded, span), 0) - WINDOW
        column = lax.broadcasted_iota(jnp.int32, (padded, span), 1)
        distance = jnp.abs(key_at - lax.rem(column, rows))
        key_place = me * rows + key_at
        inside = (distance <= WINDOW) & (key_place >= 0) & (key_place < n * rows)
        far = distance.astype(F32)
        member = lax.broadcasted_iota(jnp.int32, (1, span), 1) // rows
        for g in range(kvh):
            head = (t * (kvh * group) + g * group + 1 + member).astype(F32)
            slope = jnp.exp2(head * (-8.0 / QH_A))
            sink = jnp.zeros((1, span), F32)
            for u in range(group):
                sink = jnp.where(member == u, sink_ref[g * group + u], sink)
            scores = dot_nt(wkv[g, 0], qw[g]) * scale
            scores = jnp.where(inside, scores - slope * far, NEGATIVE)
            highest = jnp.maximum(jnp.max(scores, axis=0, keepdims=True), sink)
            raised = jnp.exp(scores - highest)
            bottom = jnp.sum(raised, axis=0, keepdims=True) + jnp.exp(sink - highest)
            weights = (raised * (1.0 / bottom)).astype(BF16)
            put_heads(0, g, dot_tn(wkv[g, 1], weights))
        ww_load.wait()
        for j in range(chunks):
            cols = slice(j * width, (j + 1) * width)
            proj[:, cols] = jnp.dot(attn[:, :heads_width], ww[:, cols], preferred_element_type=F32)

    if n > 1:
        relay(1)
    windowed()
    if n <= 4:
        for d in range(2, n):
            relay(d)
    else:
        def relay_step(d, carry):
            relay(d)
            return carry

        lax.fori_loop(2, n, relay_step, 0)

    for g in range(kvh):
        put_heads(heads_width, g, acc[g] * (1.0 / total[g]))
    gw_load.wait()

    def pair_copy(j):
        return pltpu.make_async_remote_copy(
            src_ref=pbuf.at[j, 1 - core],
            dst_ref=dbuf.at[j],
            send_sem=dsend.at[j],
            recv_sem=drecv.at[j],
            device_id={"tp": partner},
            device_id_type=MESH,
        )

    def cross_copy(j, dx):
        return pltpu.make_async_remote_copy(
            src_ref=sbuf.at[j, dx - 1],
            dst_ref=rbuf.at[j, dx - 1],
            send_sem=xsend.at[j, dx - 1],
            recv_sem=xrecv.at[j, dx - 1],
            device_id={"tp": lax.rem(x + dx, n_x) * 2 + core},
            device_id_type=MESH,
        )

    def pass_on(j):
        pair_copy(j).wait_recv()
        for dx in range(1, n_x):
            other = lax.rem(x + dx, n_x)
            sbuf[j, dx - 1] = (pbuf[j, core, other].astype(F32) + dbuf[j, other].astype(F32)).astype(BF16)
            cross_copy(j, dx).start()
        own[j] = pbuf[j, core, x].astype(F32) + dbuf[j, x].astype(F32)

    for j in range(chunks):
        cols = slice(j * width, (j + 1) * width)
        part = proj[:, cols] + jnp.dot(attn[:, heads_width:], gw[:, cols], preferred_element_type=F32)
        for b in range(n_tp):
            pbuf[j, b % 2, b // 2] = part[b * out_rows : (b + 1) * out_rows].astype(BF16)
        pair_copy(j).start()
        if j >= 1:
            pass_on(j - 1)
    pass_on(chunks - 1)
    for j in range(chunks):
        value = own[j]
        for dx in range(1, n_x):
            cross_copy(j, dx).wait_recv()
            value = value + rbuf[j, dx - 1].astype(F32)
        out_ref[:, j * width : (j + 1) * width] = value.astype(BF16)

    for j in range(chunks):
        pair_copy(j).wait_send()
        for dx in range(1, n_x):
            cross_copy(j, dx).wait_send()

    @pl.when(has_right)
    def _():
        halo_copy(0).wait_send()

    @pl.when(has_left)
    def _():
        halo_copy(1).wait_send()

    def drain(source, carry):
        for g in range(kvh):
            @pl.when(has_right & (source <= me))
            def _():
                block_copy(source, g, 0).wait_send()

            @pl.when(has_left & (source >= me))
            def _():
                block_copy(source, g, 1).wait_send()

        return carry

    lax.fori_loop(0, n, drain, 0)


def solution(mesh):
    n, n_tp = mesh.shape["sp"], mesh.shape["tp"]

    def per_device(wq, wk, wv, gq, gk, gv, sink, qgain, kgain, ww, gw):
        rows = wq.shape[0]
        kvh = wk.shape[1] // HEAD
        group = wq.shape[1] // wk.shape[1]
        model = ww.shape[1]
        chunks = 8
        width = model // chunks
        n_x = n_tp // 2
        out_rows = rows // n_tp
        heads_width = kvh * group * HEAD
        span = group * rows
        any_spec = pl.BlockSpec(memory_space=pl.ANY)
        vmem = pl.BlockSpec(memory_space=pltpu.VMEM)
        smem = pl.BlockSpec(memory_space=pltpu.SMEM)
        cross = max(n_x - 1, 1)
        return pl.pallas_call(
            functools.partial(kernel, n, n_tp, rows, kvh, group, chunks),
            out_shape=jax.ShapeDtypeStruct((out_rows, model), BF16),
            in_specs=[any_spec] * 6 + [smem, vmem, vmem, any_spec, any_spec],
            out_specs=vmem,
            scratch_shapes=[
                pltpu.VMEM((kvh, span, HEAD), BF16),
                pltpu.VMEM((kvh, 2, rows + 2 * WINDOW, HEAD), BF16),
                pltpu.VMEM((kvh, span, HEAD), BF16),
                pltpu.VMEM((kvh, rows, HEAD), BF16),
                pltpu.VMEM((kvh, span, HEAD), BF16),
                pltpu.VMEM((n, kvh, 2, rows, HEAD), BF16),
                pltpu.VMEM(ww.shape, BF16),
                pltpu.VMEM(gw.shape, BF16),
                pltpu.VMEM((rows, HEAD), F32),
                pltpu.VMEM((rows, HEAD), F32),
                pltpu.VMEM((kvh, 1, span), F32),
                pltpu.VMEM((kvh, 1, span), F32),
                pltpu.VMEM((kvh, HEAD, span), F32),
                pltpu.VMEM((rows, 2 * heads_width), BF16),
                pltpu.VMEM((rows, model), F32),
                pltpu.VMEM((chunks, 2, n_x, out_rows, width), BF16),
                pltpu.VMEM((chunks, n_x, out_rows, width), BF16),
                pltpu.VMEM((chunks, cross, out_rows, width), BF16),
                pltpu.VMEM((chunks, cross, out_rows, width), BF16),
                pltpu.VMEM((chunks, out_rows, width), F32),
                pltpu.SemaphoreType.DMA((4 * kvh + 2 * kvh * group + 2,)),
                pltpu.SemaphoreType.DMA((2, n, kvh)),
                pltpu.SemaphoreType.DMA((n, kvh)),
                pltpu.SemaphoreType.DMA((2,)),
                pltpu.SemaphoreType.DMA((2,)),
                pltpu.SemaphoreType.DMA((chunks,)),
                pltpu.SemaphoreType.DMA((chunks,)),
                pltpu.SemaphoreType.DMA((chunks, cross)),
                pltpu.SemaphoreType.DMA((chunks, cross)),
            ],
            compiler_params=pltpu.CompilerParams(
                collective_id=0, has_side_effects=True, vmem_limit_bytes=60 * 1024 * 1024
            ),
            name="hybrid",
        )(wq, wk, wv, gq, gk, gv, sink, qgain.reshape(1, HEAD), kgain.reshape(1, HEAD), ww, gw)

    return jax.shard_map(
        per_device,
        mesh=mesh,
        in_specs=(P(("grp", "sp"), "tp"),) * 6 + (P("tp"), P(), P(), P("tp", None), P("tp", None)),
        out_specs=P(("grp", "sp", "tp"), None),
        check_vma=False,
    )
```

time: 127 us -> 51.7 us (0.41)
  Pallas kernels: 0 us -> 49.6 us
  blocking collectives: 34 us -> 0 us
  waiting for transfers between devices: 33.1 us -> 0 us
  matrix products: 17.3 us -> 0 us
  other arithmetic: 15.2 us -> 0 us
  between operations: 13.9 us -> 0.01 us
  starting transfers between devices: 6.87 us -> 0 us
  local copies, waits for them, and re-layouts: 5.81 us -> 1.97 us
    pallas_call x0 -> x1, Pallas kernels: none -> 49.6 us  [per_device(): pl.pallas_call(functools.partial(kernel, n, n_tp, rows, kvh, group, chunk...]
    all_gather x2 -> x0, blocking collectives: 34 us -> none  [the longest x1 17.3 us: per_device(): lax.all_gather(turned_k, 'sp', axis=0, tiled=True)]
    reduce_scatter x1 -> x0, waiting for transfers between devices: 33.1 us -> none  [per_device(): lax.psum_scatter((projected + jnp.einsum('kgtd,kgdo->to', grid_out, shape...]
    dot_general x8 -> x0, matrix products: 17.3 us -> none  [the longest x1 6.78 us: per_device(): jnp.dot(window_out, window_weights, preferred_element_type=jnp.float32)]
    ppermute x2 -> x0, starting transfers between devices: 6.87 us -> none  [the longest x1 5.59 us: extended(): lax.ppermute(tail, axis, [(i, (i + 1) % count) for i in range(ends)])]
    another operation x3 -> x0, other arithmetic: 3.89 us -> none
    reduce_sum x5 -> x0, other arithmetic: 3.45 us -> none  [the longest x2 1.95 us: absorb_keys(): summed = summed * fading + jnp.sum(raised, axis=-1)]
    concatenate x3 -> x0, other arithmetic: 2.58 us -> none  [the longest x2 2.52 us: normed_turn(): jnp.concatenate([turn_section(scaled[..., :section], grid_row), turn_sect...]
  transfers between devices with their start and end apart: 3 -> 0, of which waited for: 1 -> 0; matrix products, arithmetic and copies ran while one was open for 21% -> 0% of each run, Pallas kernels for 0% -> 0%
where the time goes in v1:
time: 51.7 us; the launch traced here: 51.6 us
  Pallas kernels  49.6 us (96%)
  local copies, waits for them, and re-layouts  1.97 us (4%)
    pallas_call x1, Pallas kernels, per_device(): pl.pallas_call(functools.partial(kernel, n, n_tp, rows, kvh, group, chunk...  49.6 us
    unnamed x1, local copies, waits for them, and re-layouts  1.97 us

profile of v1, /device:TPU:0, one launch (start us, length us, event | category | flops | bytes accessed | tf_op | source)
XLA Modules:
  0.0 51.6 jit_solution(1351477151606443794)
XLA Ops:
  0.0 49.6 %hybrid.1 = bf16[80,4096]{1,0:T(8,128)(2,1)} custom-call(bf16[320,512]{1,0:T(8,128)(2,1)} %wq_hbm.1, bf16[320,256]{1,0:T(8,128)(2,1)} %wk_hbm.1, bf16[320,256]{1,0:T(8,128)(2,1)} %wv_hbm.1, bf16[320,512]{1,0:T(8,128)(2,1)} %gq_hbm.1, bf16[320,256]{1,0:T(8,128)(2,1)} %gk_hbm.1, bf16[320,256]{1,0:T(8,128)(2,1)} %gv_hbm.1, f32[4]{0:T(128)} %sink_ref.1, ...), custom_call_target="tpu_custom_call" | custom-call | tf_op jit(solution)/shard_map/hybrid/pallas_call | solution.py:382
  49.6 2.0 %copy.13 = bf16[80,4096]{1,0:T(8,128)(2,1)} copy(bf16[80,4096]{1,0:T(8,128)(2,1)} %hybrid.1) | data formatting | bytes 1310720

commit v2 on v1

--- a/solution.py
+++ b/solution.py
@@ -31,9 +31,9 @@
 def kernel(
     n, n_tp, rows, kvh, group, chunks,
     wq_hbm, wk_hbm, wv_hbm, gq_hbm, gk_hbm, gv_hbm, sink_ref, qgain_ref, kgain_ref, ww_hbm, gw_hbm,
-    out_ref,
-    qw, wkv, qraw, kraw, qg, kvbuf, ww, gw, cosine, sine, top, total, acc, attn, proj, pbuf, dbuf, sbuf, rbuf, own,
-    lsem, gsend, grecv, hsend, hrecv, dsend, drecv, xsend, xrecv,
+    out_hbm,
+    qw, wkv, qraw, kraw, qg, kvbuf, ww, gw, cosine, sine, top, total, acc, attn, proj, pbuf, dbuf, sbuf, rbuf, own, out_ref,
+    lsem, gsend, grecv, hsend, hrecv, dsend, drecv, xsend, xrecv, osem,
 ):
     me = lax.axis_index("sp")
     t = lax.axis_index("tp")
@@ -92,42 +92,17 @@
     for dx in range(1, n_x):
         greet({"tp": lax.rem(x + dx, n_x) * 2 + core})
 
-    place = me * rows + lax.broadcasted_iota(jnp.int32, (rows, HEAD), 0)
-    lane = lax.broadcasted_iota(jnp.int32, (rows, HEAD), 1)
-    section = HEAD // 2
-    half = section // 2
-    frequency = jnp.exp(jnp.bitwise_and(lane, half - 1).astype(F32) * (-2.0 * math.log(THETA) / section))
-    position = jnp.where(lane < section, place // GRID_W, lax.rem(place, GRID_W)).astype(F32)
-    angle = position * frequency
-    low = jnp.bitwise_and(lane, section - 1) < half
-    cosine[...] = jnp.cos(angle)
-    sine[...] = jnp.where(low, -jnp.sin(angle), jnp.sin(angle))
-
-    def turn(values, gain):
-        v = values.astype(F32)
-        v = v * lax.rsqrt(jnp.mean(v * v, axis=1, keepdims=True) + EPSILON) * gain
-        first = lax.broadcasted_iota(jnp.int32, v.shape, 1)
-        other = jnp.where(
-            jnp.bitwise_and(first, section - 1) < half,
-            pltpu.roll(v, HEAD - half, 1),
-            pltpu.roll(v, half, 1),
-        )
-        return (v * cosine[...] + other * sine[...]).astype(BF16)
-
-    for g in range(kvh):
-        k_loads[g].wait()
-        kvbuf[me, g, 0] = turn(kraw[g], kgain_ref[...])
     for copy in v_loads:
         copy.wait()
 
     pl.semaphore_wait(barrier, has_left.astype(jnp.int32) + has_right.astype(jnp.int32) + n_x)
 
-    def block_copy(source, g, direction):
+    def block_copy(source, g, kind, direction):
         return pltpu.make_async_remote_copy(
-            src_ref=kvbuf.at[source, g],
-            dst_ref=kvbuf.at[source, g],
-            send_sem=gsend.at[direction, source, g],
-            recv_sem=grecv.at[source, g],
+            src_ref=kvbuf.at[source, g, kind],
+            dst_ref=kvbuf.at[source, g, kind],
+            send_sem=gsend.at[direction, source, g, kind],
+            recv_sem=grecv.at[source, g, kind],
             device_id={"sp": me + 1 if direction == 0 else me - 1},
             device_id_type=MESH,
         )
@@ -144,14 +119,44 @@
             device_id_type=MESH,
         )
 
-    for g in range(kvh):
+    def send_own(g, kind):
         @pl.when(has_right)
         def _():
-            block_copy(me, g, 0).start()
+            block_copy(me, g, kind, 0).start()
 
         @pl.when(has_left)
         def _():
-            block_copy(me, g, 1).start()
+            block_copy(me, g, kind, 1).start()
+
+    for g in range(kvh):
+        send_own(g, 1)
+
+    place = me * rows + lax.broadcasted_iota(jnp.int32, (rows, HEAD), 0)
+    lane = lax.broadcasted_iota(jnp.int32, (rows, HEAD), 1)
+    section = HEAD // 2
+    half = section // 2
+    frequency = jnp.exp(jnp.bitwise_and(lane, half - 1).astype(F32) * (-2.0 * math.log(THETA) / section))
+    position = jnp.where(lane < section, place // GRID_W, lax.rem(place, GRID_W)).astype(F32)
+    angle = position * frequency
+    low = jnp.bitwise_and(lane, section - 1) < half
+    cosine[...] = jnp.cos(angle)
+    sine[...] = jnp.where(low, -jnp.sin(angle), jnp.sin(angle))
+
+    def turn(values, gain):
+        v = values.astype(F32)
+        v = v * lax.rsqrt(jnp.mean(v * v, axis=1, keepdims=True) + EPSILON) * gain
+        first = lax.broadcasted_iota(jnp.int32, v.shape, 1)
+        other = jnp.where(
+            jnp.bitwise_and(first, section - 1) < half,
+            pltpu.roll(v, HEAD - half, 1),
+            pltpu.roll(v, half, 1),
+        )
+        return (v * cosine[...] + other * sine[...]).astype(BF16)
+
+    for g in range(kvh):
+        k_loads[g].wait()
+        kvbuf[me, g, 0] = turn(kraw[g], kgain_ref[...])
+        send_own(g, 0)
 
     for copy in w_loads:
         copy.wait()
@@ -201,23 +206,28 @@
     for g in range(kvh):
         absorb(me, g, True)
 
+    def hand_on(d, g, kind):
+        @pl.when(me - d >= 0)
+        def _():
+            block_copy(me - d, g, kind, 0).wait_recv()
+
+            @pl.when(has_right)
+            def _():
+                block_copy(me - d, g, kind, 0).start()
+
+        @pl.when(me + d < n)
+        def _():
+            block_copy(me + d, g, kind, 1).wait_recv()
+
+            @pl.when(has_left)
+            def _():
+                block_copy(me + d, g, kind, 1).start()
+
     def relay(d):
         for g in range(kvh):
-            @pl.when(me - d >= 0)
-            def _():
-                block_copy(me - d, g, 0).wait_recv()
-
-                @pl.when(has_right)
-                def _():
-                    block_copy(me - d, g, 0).start()
-
-            @pl.when(me + d < n)
-            def _():
-                block_copy(me + d, g, 1).wait_recv()
-
-                @pl.when(has_left)
-                def _():
-                    block_copy(me + d, g, 1).start()
+            hand_on(d, g, 1)
+        for g in range(kvh):
+            hand_on(d, g, 0)
 
             @pl.when(me - d >= 0)
             def _():
@@ -326,14 +336,21 @@
         if j >= 1:
             pass_on(j - 1)
     pass_on(chunks - 1)
+
+    def out_copy(j):
+        cols = slice(j * width, (j + 1) * width)
+        return pltpu.make_async_copy(out_ref.at[:, cols], out_hbm.at[:, cols], osem.at[j])
+
     for j in range(chunks):
         value = own[j]
         for dx in range(1, n_x):
             cross_copy(j, dx).wait_recv()
             value = value + rbuf[j, dx - 1].astype(F32)
         out_ref[:, j * width : (j + 1) * width] = value.astype(BF16)
+        out_copy(j).start()
 
     for j in range(chunks):
+        out_copy(j).wait()
         pair_copy(j).wait_send()
         for dx in range(1, n_x):
             cross_copy(j, dx).wait_send()
@@ -348,13 +365,14 @@
 
     def drain(source, carry):
         for g in range(kvh):
-            @pl.when(has_right & (source <= me))
-            def _():
-                block_copy(source, g, 0).wait_send()
-
-            @pl.when(has_left & (source >= me))
-            def _():
-                block_copy(source, g, 1).wait_send()
+            for kind in range(2):
+                @pl.when(has_right & (source <= me))
+                def _():
+                    block_copy(source, g, kind, 0).wait_send()
+
+                @pl.when(has_left & (source >= me))
+                def _():
+                    block_copy(source, g, kind, 1).wait_send()
 
         return carry
 
@@ -383,7 +401,7 @@
             functools.partial(kernel, n, n_tp, rows, kvh, group, chunks),
             out_shape=jax.ShapeDtypeStruct((out_rows, model), BF16),
             in_specs=[any_spec] * 6 + [smem, vmem, vmem, any_spec, any_spec],
-            out_specs=vmem,
+            out_specs=any_spec,
             scratch_shapes=[
                 pltpu.VMEM((kvh, span, HEAD), BF16),
                 pltpu.VMEM((kvh, 2, rows + 2 * WINDOW, HEAD), BF16),
@@ -405,15 +423,17 @@
                 pltpu.VMEM((chunks, cross, out_rows, width), BF16),
                 pltpu.VMEM((chunks, cross, out_rows, width), BF16),
                 pltpu.VMEM((chunks, out_rows, width), F32),
+                pltpu.VMEM((out_rows, model), BF16),
                 pltpu.SemaphoreType.DMA((4 * kvh + 2 * kvh * group + 2,)),
-                pltpu.SemaphoreType.DMA((2, n, kvh)),
-                pltpu.SemaphoreType.DMA((n, kvh)),
+                pltpu.SemaphoreType.DMA((2, n, kvh, 2)),
+                pltpu.SemaphoreType.DMA((n, kvh, 2)),
                 pltpu.SemaphoreType.DMA((2,)),
                 pltpu.SemaphoreType.DMA((2,)),
                 pltpu.SemaphoreType.DMA((chunks,)),
                 pltpu.SemaphoreType.DMA((chunks,)),
                 pltpu.SemaphoreType.DMA((chunks, cross)),
                 pltpu.SemaphoreType.DMA((chunks, cross)),
+                pltpu.SemaphoreType.DMA((chunks,)),
             ],
             compiler_params=pltpu.CompilerParams(
                 collective_id=0, has_side_effects=True, vmem_limit_bytes=60 * 1024 * 1024

time: 51.7 us -> 51.8 us (level)
  no operation moved by 1% of the time
where the time goes in v2:
time: 51.8 us; the launch traced here: 51.6 us
  Pallas kernels  49.7 us (96%)
  local copies, waits for them, and re-layouts  1.97 us (4%)
    pallas_call x1, Pallas kernels, per_device(): pl.pallas_call(functools.partial(kernel, n, n_tp, rows, kvh, group, chunk...  49.7 us
    unnamed x1, local copies, waits for them, and re-layouts  1.97 us

profile of v2, /device:TPU:0, one launch (start us, length us, event | category | flops | bytes accessed | tf_op | source)
XLA Modules:
  0.0 51.6 jit_solution(10252537552100477684)
XLA Ops:
  0.0 49.7 %hybrid.1 = bf16[80,4096]{1,0:T(8,128)(2,1)} custom-call(bf16[320,512]{1,0:T(8,128)(2,1)} %wq_hbm.1, bf16[320,256]{1,0:T(8,128)(2,1)} %wk_hbm.1, bf16[320,256]{1,0:T(8,128)(2,1)} %wv_hbm.1, bf16[320,512]{1,0:T(8,128)(2,1)} %gq_hbm.1, bf16[320,256]{1,0:T(8,128)(2,1)} %gk_hbm.1, bf16[320,256]{1,0:T(8,128)(2,1)} %gv_hbm.1, f32[4]{0:T(128)} %sink_ref.1, ...), custom_call_target="tpu_custom_call" | custom-call | tf_op jit(solution)/shard_map/hybrid/pallas_call | solution.py:400
  49.7 2.0 %copy.13 = bf16[80,4096]{1,0:T(8,128)(2,1)} copy(bf16[80,4096]{1,0:T(8,128)(2,1)} %hybrid.1) | data formatting | bytes 1310720

commit v3 on v2

--- a/solution.py
+++ b/solution.py
@@ -139,8 +139,9 @@
     position = jnp.where(lane < section, place // GRID_W, lax.rem(place, GRID_W)).astype(F32)
     angle = position * frequency
     low = jnp.bitwise_and(lane, section - 1) < half
-    cosine[...] = jnp.cos(angle)
-    sine[...] = jnp.where(low, -jnp.sin(angle), jnp.sin(angle))
+    both = jnp.cos(jnp.where(low, angle, angle - 0.5 * math.pi))
+    cosine[...] = jnp.where(low, both, pltpu.roll(both, half, 1))
+    sine[...] = jnp.where(low, -pltpu.roll(both, HEAD - half, 1), both)
 
     def turn(values, gain):
         v = values.astype(F32)

time: 51.8 us -> 52.4 us (1.012)
    pallas_call x1, Pallas kernels: 49.7 us -> 50.2 us  [per_device(): pl.pallas_call(functools.partial(kernel, n, n_tp, rows, kvh, group, chunk...]
where the time goes in v3:
time: 52.4 us; the launch traced here: 52.2 us
  Pallas kernels  50.2 us (96%)
  local copies, waits for them, and re-layouts  1.97 us (4%)
    pallas_call x1, Pallas kernels, per_device(): pl.pallas_call(functools.partial(kernel, n, n_tp, rows, kvh, group, chunk...  50.2 us
    unnamed x1, local copies, waits for them, and re-layouts  1.97 us

profile of v3, /device:TPU:0, one launch (start us, length us, event | category | flops | bytes accessed | tf_op | source)
XLA Modules:
  0.0 52.2 jit_solution(7431548535056760961)
XLA Ops:
  0.0 50.2 %hybrid.1 = bf16[80,4096]{1,0:T(8,128)(2,1)} custom-call(bf16[320,512]{1,0:T(8,128)(2,1)} %wq_hbm.1, bf16[320,256]{1,0:T(8,128)(2,1)} %wk_hbm.1, bf16[320,256]{1,0:T(8,128)(2,1)} %wv_hbm.1, bf16[320,512]{1,0:T(8,128)(2,1)} %gq_hbm.1, bf16[320,256]{1,0:T(8,128)(2,1)} %gk_hbm.1, bf16[320,256]{1,0:T(8,128)(2,1)} %gv_hbm.1, f32[4]{0:T(128)} %sink_ref.1, ...), custom_call_target="tpu_custom_call" | custom-call | tf_op jit(solution)/shard_map/hybrid/pallas_call | solution.py:401
  50.2 2.0 %copy.13 = bf16[80,4096]{1,0:T(8,128)(2,1)} copy(bf16[80,4096]{1,0:T(8,128)(2,1)} %hybrid.1) | data formatting | bytes 1310720
